TPU v7x, 32 devices: a whole 2x2x4 slice. The times are simulated.
32 devices in a mesh: sp: 8 (over z, core), tp: 4 (over y, x).
Axes of the slice: x: 2, y: 2, z: 4, core: 2. Of those that a mesh axis runs over, the one named last changes fastest.
Arguments:
- query_rows: bfloat16 [2048, 2048], P('sp', 'tp'), may hold values from -1000 to 1000
- key_rows: bfloat16 [2048, 256], P('sp'), may hold values from -6 to 6
- value_rows: bfloat16 [2048, 256], P('sp'), may hold values from -6 to 6
- sink_logits: float32 [32], P('tp'), may hold values from 1 to 6
- out_weight: bfloat16 [2048, 2048], P('tp'), may hold values from -0.375 to 0.375
- stream_in: bfloat16 [2048, 2048], P('sp'), may hold values from -6 to 6
- norm_gain: float32 [2048], replicated, may hold values from 0.1 to 1.9
- routes: int32 [2048, 2], P('sp'), may hold values from 0 to 7, all different within a row; in each aligned block of 256 rows (0 to 255, 256 to 511, ...) at most 96 rows name the same one
- route_weights: float32 [2048, 2], P('sp'), may hold values from 0.2 to 1
- gate_weight: bfloat16 [8, 2048, 4096], P('sp', None, 'tp'), may hold values from -0.125 to 0.125
- up_weight: bfloat16 [8, 2048, 4096], P('sp', None, 'tp'), may hold values from -0.125 to 0.125
- down_weight: bfloat16 [8, 4096, 2048], P('sp', 'tp'), may hold values from -0.09375 to 0.09375
Outputs:
- layer_out: bfloat16 [2048, 2048], P(('sp', 'tp'))
Inputs may be any that keep to these rules, and one draw needn't show every extreme that they name: `routes`: each row names 2 different experts. Within the rows of one device (256 aligned rows) no expert is named more than 96 times, a bound that some block reaches.
All inputs are finite; a program needn't handle non-finite values.
Results may differ from a plain program's by a relative error of at most 0.015.
Values may be sent and summed in bfloat16 or wider, within the bound.
A program may use at most 64 MiB of HBM per device.

v0:
```python
import jax
import jax.numpy as jnp
from jax import lax
from jax.sharding import PartitionSpec as P

HEAD_DIM = 64
REP = 8
WINDOW = 128
norm_eps = 1e-06


def shifted(block, axis, distance):
    devices = range(lax.axis_size(axis))
    route = [(i - distance, i) for i in devices if i - distance in devices]
    return lax.ppermute(block, axis, route)


def rms_scale(stream, norm_gain):
    values = stream.astype(jnp.float32)
    scaled = values * lax.rsqrt(jnp.mean(values * values, axis=-1, keepdims=True) + norm_eps)
    return (scaled * norm_gain).astype(jnp.bfloat16)


def slot_tables(routes, experts_n, slot_cap):
    flat_ids = routes.reshape(-1)
    onehot = (flat_ids[:, None] == jnp.arange(experts_n, dtype=jnp.int32)[None, :]).astype(
        jnp.int32
    )
    before = jnp.cumsum(onehot, axis=0) - onehot
    targets = flat_ids * slot_cap + jnp.sum(before * onehot, axis=1)
    pair_token = jnp.arange(flat_ids.shape[0], dtype=jnp.int32) // routes.shape[1]
    slot_token = jnp.zeros((experts_n * slot_cap,), jnp.int32).at[targets].set(pair_token)
    slot_live = jnp.zeros((experts_n * slot_cap,), jnp.int32).at[targets].set(1)
    return (targets, slot_token, slot_live)


def per_device(
    query_rows,
    key_rows,
    value_rows,
    sink_logits,
    out_weight,
    stream_in,
    norm_gain,
    routes,
    route_weights,
    gate_weight,
    up_weight,
    down_weight,
):
    tok_count = query_rows.shape[0]
    local_heads = query_rows.shape[1] // HEAD_DIM
    tp_index = lax.axis_index("tp")
    kv_group = tp_index * local_heads // REP
    own_keys = lax.dynamic_slice_in_dim(key_rows, kv_group * HEAD_DIM, HEAD_DIM, 1)
    own_values = lax.dynamic_slice_in_dim(value_rows, kv_group * HEAD_DIM, HEAD_DIM, 1)
    prior_keys, prior_values = shifted(
        (own_keys[tok_count - WINDOW :], own_values[tok_count - WINDOW :]), "sp", 1
    )
    key_block = jnp.concatenate([prior_keys, own_keys], axis=0)
    value_block = jnp.concatenate([prior_values, own_values], axis=0)
    offset = lax.axis_index("sp") * tok_count
    query_pos = offset + jnp.arange(tok_count, dtype=jnp.int32)
    key_pos = offset - WINDOW + jnp.arange(tok_count + WINDOW, dtype=jnp.int32)
    distance = query_pos[:, None] - key_pos[None, :]
    allowed = (distance >= 0) & (distance < WINDOW) & (key_pos >= 0)[None, :]
    queries = query_rows.reshape(tok_count, local_heads, HEAD_DIM)
    scores = jnp.einsum(
        "qhd,kd->hqk", queries, key_block, preferred_element_type=jnp.float32
    ) * HEAD_DIM ** (-0.5)
    scores = jnp.where(allowed[None], scores, -1e30)
    sink_col = sink_logits.reshape(local_heads, 1, 1)
    row_peak = jnp.maximum(jnp.max(scores, axis=-1, keepdims=True), sink_col)
    exp_terms = jnp.exp(scores - row_peak)
    denom_sum = jnp.sum(exp_terms, axis=-1, keepdims=True) + jnp.exp(sink_col - row_peak)
    attn_probs = (exp_terms / denom_sum).astype(jnp.bfloat16)
    attended = jnp.einsum(
        "hqk,kd->qhd", attn_probs, value_block, preferred_element_type=jnp.float32
    )
    attended = attended.astype(jnp.bfloat16).reshape(tok_count, local_heads * HEAD_DIM)
    row_share = tok_count // lax.axis_size("tp")
    projected = lax.psum(
        jnp.dot(attended, out_weight, preferred_element_type=jnp.float32).astype(jnp.bfloat16), "tp"
    ).astype(jnp.float32)
    stream = (stream_in.astype(jnp.float32) + projected).astype(jnp.bfloat16)
    normed_all = rms_scale(stream, norm_gain)
    own_stream = lax.dynamic_slice_in_dim(stream, tp_index * row_share, row_share, 0)
    experts_n = lax.axis_size("sp")
    top_count = routes.shape[1]
    slot_cap = 3 * tok_count * top_count // (2 * experts_n)
    targets, slot_token, slot_live = slot_tables(routes, experts_n, slot_cap)
    width_share = normed_all.shape[1] // lax.axis_size("tp")
    columns = lax.dynamic_slice_in_dim(normed_all, tp_index * width_share, width_share, 1)
    outgoing = jnp.where(slot_live[:, None] > 0, columns[slot_token], jnp.zeros((), jnp.bfloat16))
    outgoing = outgoing.reshape(experts_n, slot_cap, width_share)
    arrived = lax.all_to_all(outgoing, "sp", split_axis=0, concat_axis=0, tiled=True)
    arrived = lax.all_gather(arrived, "tp", axis=2, tiled=True)
    sources = arrived.shape[0]
    item_count = arrived.shape[1]
    flat_rows = arrived.reshape(sources * item_count, arrived.shape[2])
    gate_act = jnp.dot(flat_rows, gate_weight[0], preferred_element_type=jnp.float32)
    up_act = jnp.dot(flat_rows, up_weight[0], preferred_element_type=jnp.float32)
    hidden = (jax.nn.silu(gate_act) * up_act).astype(jnp.bfloat16)
    partial_value = jnp.dot(hidden, down_weight[0], preferred_element_type=jnp.float32).astype(
        jnp.bfloat16
    )
    partial_value = partial_value.reshape(sources, item_count, partial_value.shape[1])
    returned = lax.all_to_all(partial_value, "sp", split_axis=0, concat_axis=0, tiled=True)
    returned_flat = returned.reshape(experts_n * slot_cap, returned.shape[2])
    pair_weights = route_weights.reshape(-1)
    chosen = returned_flat[targets].astype(jnp.float32) * pair_weights[:, None]
    moe_rows = lax.psum_scatter(
        jnp.sum(
            chosen.reshape(row_share * lax.axis_size("tp"), top_count, chosen.shape[1]), axis=1
        ).astype(jnp.bfloat16),
        "tp",
        scatter_dimension=0,
        tiled=True,
    ).astype(jnp.float32)
    return (own_stream.astype(jnp.float32) + moe_rows).astype(jnp.bfloat16)


def solution(mesh):
    return jax.shard_map(
        per_device,
        mesh=mesh,
        in_specs=(
            P("sp", "tp"),
            P("sp", None),
            P("sp", None),
            P("tp"),
            P("tp", None),
            P("sp", None),
            P(),
            P("sp", None),
            P("sp", None),
            P("sp", None, "tp"),
            P("sp", None, "tp"),
            P("sp", "tp", None),
        ),
        out_specs=P(("sp", "tp"), None),
        check_vma=False,
    )
```

profile of v0, /device:TPU:0, one launch (start us, length us, event | category | flops | bytes accessed | tf_op | source)
XLA Modules:
  0.0 299.9 jit_solution(17080001785737628045)
XLA Ops:
  6.5 0.0 copy-start
  6.5 0.0 copy-start.2
  6.5 0.0 all-reduce.2.cloned.1.call-start
  6.5 1.1 constant_dynamic-slice_fusion
  7.6 0.1 copy.28
  7.7 2.4 collective-permute-start.1
  10.1 0.9 constant_dynamic-slice_fusion.1
  11.1 0.1 copy.27
  11.2 4.6 %collective-permute-start = (bf16[128,64]{0,1:T(8,128)(2,1)S(1)}, bf16[128,64]{0,1:T(8,128)(2,1)S(1)}, u32[]{:S(2)}, u32[]{:S(2)}) collective-permute-start(bf16[128,64]{0,1:T(8,128)(2,1)S(1)} %slice.20), channel_id=1, source_target_pairs={{0,4},{4,8},{8,12},{12,16},{16,20},{20,24},{24,28},{1,5},{5,9},{9,... | collective-permute-start | bytes 49160 | tf_op jit(solution)/shard_map/ppermute | solution.py:15
  15.8 0.8 copy.23
  16.6 0.1 eq.29
  16.8 0.2 fusion.18
  17.0 0.7 broadcast_multiply_fusion
  17.7 1.1 copy.20
  18.8 1.1 reduce-window.6
  19.9 0.0 collective-permute-done.1
  19.9 0.7 fusion.10
  20.6 0.0 copy-done.2
  20.6 0.1 broadcast_maximum_fusion
  20.7 0.7 fusion.9
  21.3 0.1 exponential_add_fusion
  21.4 0.0 collective-permute-done
  21.4 1.0 fusion.14
  22.4 0.0 copy-done
  22.4 1.8 convolution_convert_fusion
  24.2 0.0 all-reduce.2.cloned.1.call-update
  24.2 0.0 all-gather.2.cloned.1.call-start
  24.2 0.2 slice_reduce_fusion
  24.5 0.1 eq.25
  24.6 0.1 copy.22
  24.8 0.1 mul.88
  24.9 0.1 fusion.25
  25.0 2.4 scatter_custom_fusion.1
  27.5 2.4 scatter_custom_fusion
  30.0 0.1 broadcast_in_dim.48
  30.1 0.8 dynamic-slice
  30.8 46.2 %all-reduce.2.cloned.1.call-done = bf16[256,2048]{1,0:T(8,128)(2,1)} async-done(((bf16[256,2048]{1,0:T(8,128)(2,1)}), bf16[256,2048]{1,0:T(8,128)(2,1)}) %all-reduce.2.cloned.1.call-update) | async-done | bytes 1048592 | tf_op jit(solution)/shard_map/psum | solution.py:82
  77.0 2.0 multiply_reduce_fusion.1
  79.1 0.2 convert_element_type.69
  79.3 0.1 fusion.16
  79.5 3.3 %gather_fusion = bf16[768,512]{1,0:T(8,128)(2,1)} fusion(bf16[256,512]{1,0:T(8,128)(2,1)S(1)} %fusion.16, s32[1024]{0:T(1024)S(1)} %pad_clamp_fusion.1), kind=kCustom, calls=%fused_computation | custom fusion | bytes 1575936 | tf_op jit(solution)/shard_map/gather | solution.py:94
  82.8 1.3 broadcast_select_fusion
  84.1 25.5 %all_to_all.10 = bf16[8,96,512]{2,1,0:T(8,128)(2,1)} all-to-all(bf16[8,96,512]{2,1,0:T(8,128)(2,1)S(1)} %broadcast_select_fusion), channel_id=1, replica_groups=mesh['sp'=8,'tp'=4] {'sp'}, dimensions={0} | all-to-all | bytes 1572864 | tf_op jit(solution)/shard_map/all_to_all | solution.py:96
  109.5 0.0 all-gather.2.cloned.1.call-update
  109.6 41.8 %all-gather.2.cloned.1.call-done = bf16[8,96,2048]{2,1,0:T(8,128)(2,1)} async-done(((bf16[8,96,512]{2,1,0:T(8,128)(2,1)}), bf16[8,96,2048]{2,1,0:T(8,128)(2,1)}) %all-gather.2.cloned.1.call-update) | async-done | bytes 3145744 | tf_op jit(solution)/shard_map/all_gather | solution.py:97
  151.4 0.0 copy-start.3
  151.4 6.3 %fusion.2 = f32[768,1024]{1,0:T(8,128)S(1)} fusion(bf16[768,2048]{1,0:T(8,128)(2,1)} %bitcast.64, bf16[1,2048,1024]{2,1,0:T(8,128)(2,1)} %param.22), kind=kOutput, calls=%fused_computation.6 | convolution fusion | flops 3221225472 | bytes 10485760 | tf_op jit(solution)/shard_map/dot_general | solution.py:102
  157.7 0.0 copy-done.3
  157.7 0.0 copy-done.5
  157.7 0.0 copy-start.4
  157.7 3.8 %multiply_convert_fusion = bf16[768,1024]{1,0:T(8,128)(2,1)S(1)} fusion(f32[768,1024]{1,0:T(8,128)S(1)} %fusion.2, bf16[768,2048]{1,0:T(8,128)(2,1)S(1)} %bitcast.65, bf16[1,2048,1024]{2,1,0:T(8,128)(2,1)S(1)} %copy-done.3), kind=kOutput, calls=%fused_computation.13 | convolution fusion | flops 3225944064 | bytes 12058624 | tf_op jit(solution)/shard_map/dot_general | solution.py:101
  161.5 0.0 copy-done.4
  161.5 4.8 %fusion.6 = bf16[768,2048]{1,0:T(8,128)(2,1)} fusion(bf16[768,1024]{1,0:T(8,128)(2,1)S(1)} %multiply_convert_fusion, bf16[1,1024,2048]{2,1,0:T(8,128)(2,1)S(1)} %copy-done.4), kind=kOutput, calls=%fused_computation.11 | convolution fusion | flops 3222798336 | bytes 8912896 | tf_op jit(solution)/shard_map/dot_general | solution.py:104
  166.4 4.7 %all-to-all-start.1 = ((bf16[8,96,2048]{2,1,0:T(8,128)(2,1)}), bf16[8,96,2048]{2,1,0:T(8,128)(2,1)}, u32[]{:S(2)}, u32[]{:S(2)}) async-start(bf16[8,96,2048]{2,1,0:T(8,128)(2,1)} %bitcast.56), calls=%async_computation.1 | async-start | bytes 6291456 | tf_op jit(solution)/shard_map/all_to_all | solution.py:108
  171.1 0.3 reduce-scatter.2.cloned.1.call-start
  171.4 0.0 copy-done.1
  171.4 0.1 copy.25
  171.5 71.2 %all-to-all-done.1 = bf16[8,96,2048]{2,1,0:T(8,128)(2,1)} async-done(((bf16[8,96,2048]{2,1,0:T(8,128)(2,1)}), bf16[8,96,2048]{2,1,0:T(8,128)(2,1)}, u32[]{:S(2)}, u32[]{:S(2)}) %all-to-all-start.1) | async-done | bytes 3145760 | tf_op jit(solution)/shard_map/all_to_all | solution.py:108
  242.7 7.6 %gather_fusion.1 = bf16[512,2048]{1,0:T(8,128)(2,1)} fusion(bf16[768,2048]{1,0:T(8,128)(2,1)} %bitcast.16, s32[1024]{0:T(1024)S(1)} %pad_clamp_fusion), kind=kCustom, calls=%fused_computation.1 | custom fusion | bytes 4196352 | tf_op jit(solution)/shard_map/gather | solution.py:111
  250.3 5.4 %reshape.209 = f32[256,2,2048]{2,1,0:T(2,128)} reshape(bf16[512,2048]{1,0:T(8,128)(2,1)} %gather_fusion.1) | data formatting | bytes 6291456 | tf_op jit(solution)/shard_map/convert_element_type | solution.py:111
  255.7 9.9 %multiply_reduce_fusion = bf16[256,2048]{1,0:T(8,128)(2,1)} fusion(f32[256,2,2048]{2,1,0:T(2,128)} %reshape.209, f32[256,2]{1,0:T(8,128)S(1)} %copy.25), kind=kLoop, calls=%fused_computation.10 | loop fusion | flops 1572864 | bytes 5244928 | tf_op jit(solution)/shard_map/reduce_sum | solution.py:113
  265.6 0.0 reduce-scatter.2.cloned.1.call-update
  265.6 26.0 %reduce-scatter.2.cloned.1.call-done = bf16[64,2048]{1,0:T(8,128)(2,1)} async-done(((bf16[256,2048]{1,0:T(8,128)(2,1)}), bf16[64,2048]{1,0:T(8,128)(2,1)}) %reduce-scatter.2.cloned.1.call-update) | async-done | bytes 262160 | tf_op jit(solution)/shard_map/reduce_scatter | solution.py:112
  291.6 1.7 add_convert_fusion.1
  (18 shorter events, 0.1 us)
Async XLA Ops:
  6.5 15.9 %copy-start = (bf16[512,2048]{1,0:T(8,128)(2,1)S(1)}, bf16[512,2048]{1,0:T(8,128)(2,1)}, u32[]{:S(2)}) copy-start(bf16[512,2048]{1,0:T(8,128)(2,1)} %param.16) | copy-start | bytes 6291460
  6.5 14.0 %copy-start.2 = (f32[8]{0:T(128)S(1)}, f32[8]{0:T(128)}, u32[]{:S(2)}) copy-start(f32[8]{0:T(128)} %param.15) | copy-start | bytes 100
  6.5 70.5 %all-reduce.2.cloned.1.call-start = ((), (), s32[]{:S(2)}) async-start(), calls=%async_computation.3 | async-start | bytes 2097152 | tf_op jit(solution)/shard_map/psum | solution.py:82
  7.7 12.2 %collective-permute-start.1 = (bf16[128,64]{0,1:T(8,128)(2,1)S(1)}, bf16[128,64]{0,1:T(8,128)(2,1)S(1)}, u32[]{:S(2)}, u32[]{:S(2)}) collective-permute-start(bf16[128,64]{0,1:T(8,128)(2,1)S(1)} %slice.21), channel_id=1, source_target_pairs={{0,4},{4,8},{8,12},{12,16},{16,20},{20,24},{24,28},{1,5},{5,9},{9,... | collective-permute-start | bytes 49160 | tf_op jit(solution)/shard_map/ppermute | solution.py:15
  11.2 10.2 %collective-permute-start = (bf16[128,64]{0,1:T(8,128)(2,1)S(1)}, bf16[128,64]{0,1:T(8,128)(2,1)S(1)}, u32[]{:S(2)}, u32[]{:S(2)}) collective-permute-start(bf16[128,64]{0,1:T(8,128)(2,1)S(1)} %slice.20), channel_id=1, source_target_pairs={{0,4},{4,8},{8,12},{12,16},{16,20},{20,24},{24,28},{1,5},{5,9},{9,... | collective-permute-start | bytes 49160 | tf_op jit(solution)/shard_map/ppermute | solution.py:15
  24.2 127.2 %all-gather.2.cloned.1.call-start = ((), (), s32[]{:S(2)}) async-start(), calls=%async_computation.4 | async-start | bytes 3932160 | tf_op jit(solution)/shard_map/all_gather | solution.py:97
  151.4 6.3 %copy-start.3 = (bf16[1,2048,1024]{2,1,0:T(8,128)(2,1)S(1)}, bf16[1,2048,1024]{2,1,0:T(8,128)(2,1)}, u32[]{:S(2)}) copy-start(bf16[1,2048,1024]{2,1,0:T(8,128)(2,1)} %param.21) | copy-start | bytes 12582916
  151.4 6.3 %copy-start.5 = (bf16[8,96,2048]{2,1,0:T(8,128)(2,1)S(1)}, bf16[8,96,2048]{2,1,0:T(8,128)(2,1)}, u32[]{:S(2)}) copy-start(bf16[8,96,2048]{2,1,0:T(8,128)(2,1)} %all-gather.2.cloned.1.call-done) | copy-start | bytes 9437188
  157.7 3.8 %copy-start.4 = (bf16[1,1024,2048]{2,1,0:T(8,128)(2,1)S(1)}, bf16[1,1024,2048]{2,1,0:T(8,128)(2,1)}, u32[]{:S(2)}) copy-start(bf16[1,1024,2048]{2,1,0:T(8,128)(2,1)} %param.23) | copy-start | bytes 12582916
  166.4 5.0 %copy-start.1 = (f32[256,2]{0,1:T(2,128)S(1)}, f32[256,2]{0,1:T(2,128)}, u32[]{:S(2)}) copy-start(f32[256,2]{0,1:T(2,128)} %param.20) | copy-start | bytes 6148
  166.4 76.4 %all-to-all-start.1 = ((bf16[8,96,2048]{2,1,0:T(8,128)(2,1)}), bf16[8,96,2048]{2,1,0:T(8,128)(2,1)}, u32[]{:S(2)}, u32[]{:S(2)}) async-start(bf16[8,96,2048]{2,1,0:T(8,128)(2,1)} %bitcast.56), calls=%async_computation.1 | async-start | bytes 6291456 | tf_op jit(solution)/shard_map/all_to_all | solution.py:108
  171.1 120.5 %reduce-scatter.2.cloned.1.call-start = ((), (), s32[]{:S(2)}) async-start(), calls=%async_computation.5 | async-start | bytes 1310720 | tf_op jit(solution)/shard_map/reduce_scatter | solution.py:112
Sparse Core Ops, SparseCore 0:
  24.3 52.6 all-reduce.1
  109.7 41.6 all-gather.1
  265.7 25.8 reduce-scatter.1
where the time goes:
time: 301 us; the launch traced here: 300 us
  waiting for transfers between devices  185 us (61%)
  local copies, waits for them, and re-layouts  27.1 us (9%)
  blocking collectives  25.5 us (8%)
  other arithmetic  18.3 us (6%)
  matrix products  18.3 us (6%)
  between operations  13.4 us (4%)
  starting transfers between devices  12 us (4%)
    all_to_all x1, waiting for transfers between devices, per_device(): lax.all_to_all(partial_value, 'sp', split_axis=0, concat_axis=0, tiled=True)  71.2 us
    psum x1, waiting for transfers between devices, per_device(): lax.psum(jnp.dot(attended, out_weight, preferred_element_type=jnp.float32...  46.2 us
    all_gather x1, waiting for transfers between devices, per_device(): arrived = lax.all_gather(arrived, 'tp', axis=2, tiled=True)  41.8 us
    reduce_scatter x1, waiting for transfers between devices, per_device(): lax.psum_scatter(jnp.sum(chosen.reshape(row_share * lax.axis_size('tp'),...  26 us
    all_to_all x1, blocking collectives, per_device(): lax.all_to_all(outgoing, 'sp', split_axis=0, concat_axis=0, tiled=True)  25.5 us
    reduce_sum x1, other arithmetic, per_device(): jnp.sum(chosen.reshape(row_share * lax.axis_size('tp'), top_count, chosen...  9.87 us
    gather x1, local copies, waits for them, and re-layouts, per_device(): chosen = returned_flat[targets].astype(jnp.float32) * pair_weights[:, None]  7.56 us
    ppermute x2, starting transfers between devices, shifted(): return lax.ppermute(block, axis, route)  6.98 us
  transfers between devices with their start and end apart: 6, of which 4 were waited for; matrix products, arithmetic and copies ran while one was open for 4% of the time, Pallas kernels for 0%

commit v1 on v0

--- a/solution.py
+++ b/solution.py
@@ -79,7 +79,10 @@
     )
     attended = attended.astype(jnp.bfloat16).reshape(tok_count, local_heads * HEAD_DIM)
     row_share = tok_count // lax.axis_size("tp")
-    projected = lax.psum(
+    produce_shifts_all_on_mesh = lambda my_data, named_axis: lax.all_gather(
+        my_data, axis_name=named_axis
+    ).sum(axis=0)
+    projected = produce_shifts_all_on_mesh(
         jnp.dot(attended, out_weight, preferred_element_type=jnp.float32).astype(jnp.bfloat16), "tp"
     ).astype(jnp.float32)
     stream = (stream_in.astype(jnp.float32) + projected).astype(jnp.bfloat16)

time: 301 us -> 302 us (level)
  other arithmetic: 18.3 us -> 21.9 us
    psum x1 -> x0, waiting for transfers between devices: 46.2 us -> none  [per_device(): lax.psum(jnp.dot(attended, out_weight, preferred_element_type=jnp.float32...]
    all_gather x0 -> x1, waiting for transfers between devices: none -> 44.9 us  [per_device(): lax.all_gather(my_data, axis_name=named_axis).sum(axis=0)]
    reduce_sum x0 -> x1, other arithmetic: none -> 4.25 us  [per_device(): produce_shifts_all_on_mesh = lambda my_data, named_axis: lax.all_gather(m...]
where the time goes in v1:
time: 302 us; the launch traced here: 301 us
  waiting for transfers between devices  184 us (61%)
  local copies, waits for them, and re-layouts  26.4 us (9%)
  blocking collectives  25.5 us (8%)
  other arithmetic  21.9 us (7%)
  matrix products  18.2 us (6%)
  between operations  13.4 us (4%)
  starting transfers between devices  11.8 us (4%)
    all_to_all x1, waiting for transfers between devices, per_device(): lax.all_to_all(partial_value, 'sp', split_axis=0, concat_axis=0, tiled=True)  71.4 us
    all_gather x1, waiting for transfers between devices, per_device(): lax.all_gather(my_data, axis_name=named_axis).sum(axis=0)  44.9 us
    all_gather x1, waiting for transfers between devices, per_device(): arrived = lax.all_gather(arrived, 'tp', axis=2, tiled=True)  41.8 us
    reduce_scatter x1, waiting for transfers between devices, per_device(): lax.psum_scatter(jnp.sum(chosen.reshape(row_share * lax.axis_size('tp'),...  26 us
    all_to_all x1, blocking collectives, per_device(): lax.all_to_all(outgoing, 'sp', split_axis=0, concat_axis=0, tiled=True)  25.5 us
    reduce_sum x1, other arithmetic, per_device(): jnp.sum(chosen.reshape(row_share * lax.axis_size('tp'), top_count, chosen...  9.87 us
    gather x1, local copies, waits for them, and re-layouts, per_device(): chosen = returned_flat[targets].astype(jnp.float32) * pair_weights[:, None]  7.56 us
    ppermute x2, starting transfers between devices, shifted(): return lax.ppermute(block, axis, route)  6.98 us
  transfers between devices with their start and end apart: 6, of which 4 were waited for; matrix products, arithmetic and copies ran while one was open for 4% of the time, Pallas kernels for 0%

profile of v1, /device:TPU:0, one launch (start us, length us, event | category | flops | bytes accessed | tf_op | source)
XLA Modules:
  0.0 301.4 jit_solution(3139983673673870034)
XLA Ops:
  6.5 0.0 copy-start
  6.5 0.0 all-gather.6.cloned.1.call-start
  6.5 1.1 constant_dynamic-slice_fusion
  7.6 0.1 copy.28
  7.7 2.4 collective-permute-start.1
  10.1 0.9 constant_dynamic-slice_fusion.1
  11.1 0.1 copy.27
  11.2 4.6 %collective-permute-start = (bf16[128,64]{0,1:T(8,128)(2,1)S(1)}, bf16[128,64]{0,1:T(8,128)(2,1)S(1)}, u32[]{:S(2)}, u32[]{:S(2)}) collective-permute-start(bf16[128,64]{0,1:T(8,128)(2,1)S(1)} %slice.20), channel_id=1, source_target_pairs={{0,4},{4,8},{8,12},{12,16},{16,20},{20,24},{24,28},{1,5},{5,9},{9,... | collective-permute-start | bytes 49160 | tf_op jit(solution)/shard_map/ppermute | solution.py:15
  15.8 0.2 fusion.18
  16.0 1.1 copy.20
  17.1 0.0 collective-permute-done.1
  17.1 0.7 fusion.10
  17.8 0.0 copy-done.3
  17.8 0.1 broadcast_maximum_fusion
  17.9 0.7 fusion.9
  18.5 0.1 exponential_add_fusion
  18.6 0.0 collective-permute-done
  18.6 1.0 fusion.14
  19.6 0.0 copy-start.1
  19.6 0.0 copy-done
  19.6 1.7 convolution_convert_fusion
  21.3 0.0 all-gather.6.cloned.1.call-update
  21.3 0.0 all-gather.4.cloned.1.call-start
  21.4 0.0 copy-done.1
  21.4 0.1 copy.23
  21.5 0.1 eq.29
  21.7 0.1 eq.25
  21.8 1.1 reduce-window.6
  23.0 0.2 slice_reduce_fusion
  23.3 0.1 copy.22
  23.4 0.1 mul.88
  23.6 0.1 fusion.25
  23.7 2.4 scatter_custom_fusion.1
  26.1 2.4 scatter_custom_fusion
  28.6 0.1 broadcast_in_dim.48
  28.7 0.8 dynamic-slice
  29.5 44.9 %all-gather.6.cloned.1.call-done = bf16[1024,2048]{1,0:T(8,128)(2,1)} async-done(((bf16[256,2048]{1,0:T(8,128)(2,1)}), bf16[1024,2048]{1,0:T(8,128)(2,1)}) %all-gather.6.cloned.1.call-update) | async-done | bytes 4194320 | tf_op jit(solution)/shard_map/all_gather | solution.py:82
  74.3 4.3 %reduce_sum.51 = bf16[256,2048]{1,0:T(8,128)(2,1)} reduce(bf16[4,256,2048]{2,1,0:T(8,128)(2,1)} %bitcast.57, bf16[]{:T(256)} %constant.79.clone.1), dimensions={0}, to_apply=%region_2.3 | reduce | flops 1572864 | bytes 5242882 | tf_op jit(solution)/shard_map/reduce_sum | solution.py:84
  78.6 2.0 multiply_reduce_fusion.1
  80.6 0.2 convert_element_type.71
  80.9 0.1 fusion.16
  81.0 3.3 %gather_fusion = bf16[768,512]{1,0:T(8,128)(2,1)} fusion(bf16[256,512]{1,0:T(8,128)(2,1)S(1)} %fusion.16, s32[1024]{0:T(1024)S(1)} %pad_clamp_fusion.1), kind=kCustom, calls=%fused_computation | custom fusion | bytes 1575936 | tf_op jit(solution)/shard_map/gather | solution.py:97
  84.3 1.3 broadcast_select_fusion
  85.7 25.5 %all_to_all.10 = bf16[8,96,512]{2,1,0:T(8,128)(2,1)} all-to-all(bf16[8,96,512]{2,1,0:T(8,128)(2,1)S(1)} %broadcast_select_fusion), channel_id=1, replica_groups=mesh['sp'=8,'tp'=4] {'sp'}, dimensions={0} | all-to-all | bytes 1572864 | tf_op jit(solution)/shard_map/all_to_all | solution.py:99
  111.1 0.0 all-gather.4.cloned.1.call-update
  111.1 41.8 %all-gather.4.cloned.1.call-done = bf16[8,96,2048]{2,1,0:T(8,128)(2,1)} async-done(((bf16[8,96,512]{2,1,0:T(8,128)(2,1)}), bf16[8,96,2048]{2,1,0:T(8,128)(2,1)}) %all-gather.4.cloned.1.call-update) | async-done | bytes 3145744 | tf_op jit(solution)/shard_map/all_gather | solution.py:100
  153.0 6.3 %fusion.2 = f32[768,1024]{1,0:T(8,128)S(1)} fusion(bf16[768,2048]{1,0:T(8,128)(2,1)} %bitcast.66, bf16[1,2048,1024]{2,1,0:T(8,128)(2,1)} %param.22), kind=kOutput, calls=%fused_computation.6 | convolution fusion | flops 3221225472 | bytes 10485760 | tf_op jit(solution)/shard_map/dot_general | solution.py:105
  159.3 0.0 copy-done.4
  159.3 0.0 copy-done.6
  159.3 0.0 copy-start.5
  159.3 3.8 %multiply_convert_fusion = bf16[768,1024]{1,0:T(8,128)(2,1)S(1)} fusion(f32[768,1024]{1,0:T(8,128)S(1)} %fusion.2, bf16[768,2048]{1,0:T(8,128)(2,1)S(1)} %bitcast.67, bf16[1,2048,1024]{2,1,0:T(8,128)(2,1)S(1)} %copy-done.4), kind=kOutput, calls=%fused_computation.13 | convolution fusion | flops 3225944064 | bytes 12058624 | tf_op jit(solution)/shard_map/dot_general | solution.py:104
  163.1 0.0 copy-done.5
  163.1 4.8 %fusion.6 = bf16[768,2048]{1,0:T(8,128)(2,1)} fusion(bf16[768,1024]{1,0:T(8,128)(2,1)S(1)} %multiply_convert_fusion, bf16[1,1024,2048]{2,1,0:T(8,128)(2,1)S(1)} %copy-done.5), kind=kOutput, calls=%fused_computation.11 | convolution fusion | flops 3222798336 | bytes 8912896 | tf_op jit(solution)/shard_map/dot_general | solution.py:107
  167.9 4.7 %all-to-all-start.1 = ((bf16[8,96,2048]{2,1,0:T(8,128)(2,1)}), bf16[8,96,2048]{2,1,0:T(8,128)(2,1)}, u32[]{:S(2)}, u32[]{:S(2)}) async-start(bf16[8,96,2048]{2,1,0:T(8,128)(2,1)} %bitcast.58), calls=%async_computation.1 | async-start | bytes 6291456 | tf_op jit(solution)/shard_map/all_to_all | solution.py:111
  172.7 0.0 reduce-scatter.2.cloned.1.call-start
  172.7 0.0 copy-done.2
  172.7 0.1 copy.25
  172.9 71.4 %all-to-all-done.1 = bf16[8,96,2048]{2,1,0:T(8,128)(2,1)} async-done(((bf16[8,96,2048]{2,1,0:T(8,128)(2,1)}), bf16[8,96,2048]{2,1,0:T(8,128)(2,1)}, u32[]{:S(2)}, u32[]{:S(2)}) %all-to-all-start.1) | async-done | bytes 3145760 | tf_op jit(solution)/shard_map/all_to_all | solution.py:111
  244.3 7.6 %gather_fusion.1 = bf16[512,2048]{1,0:T(8,128)(2,1)} fusion(bf16[768,2048]{1,0:T(8,128)(2,1)} %bitcast.17, s32[1024]{0:T(1024)S(1)} %pad_clamp_fusion), kind=kCustom, calls=%fused_computation.1 | custom fusion | bytes 4196352 | tf_op jit(solution)/shard_map/gather | solution.py:114
  251.8 5.4 %reshape.209 = f32[256,2,2048]{2,1,0:T(2,128)} reshape(bf16[512,2048]{1,0:T(8,128)(2,1)} %gather_fusion.1) | data formatting | bytes 6291456 | tf_op jit(solution)/shard_map/convert_element_type | solution.py:114
  257.3 9.9 %multiply_reduce_fusion = bf16[256,2048]{1,0:T(8,128)(2,1)} fusion(f32[256,2,2048]{2,1,0:T(2,128)} %reshape.209, f32[256,2]{1,0:T(8,128)S(1)} %copy.25), kind=kLoop, calls=%fused_computation.10 | loop fusion | flops 1572864 | bytes 5244928 | tf_op jit(solution)/shard_map/reduce_sum | solution.py:116
  267.1 0.0 reduce-scatter.2.cloned.1.call-update
  267.2 26.0 %reduce-scatter.2.cloned.1.call-done = bf16[64,2048]{1,0:T(8,128)(2,1)} async-done(((bf16[256,2048]{1,0:T(8,128)(2,1)}), bf16[64,2048]{1,0:T(8,128)(2,1)}) %reduce-scatter.2.cloned.1.call-update) | async-done | bytes 262160 | tf_op jit(solution)/shard_map/reduce_scatter | solution.py:115
  293.2 1.7 add_convert_fusion.1
  (21 shorter events, 0.1 us)
Async XLA Ops:
  6.5 13.1 %copy-start = (bf16[512,2048]{1,0:T(8,128)(2,1)S(1)}, bf16[512,2048]{1,0:T(8,128)(2,1)}, u32[]{:S(2)}) copy-start(bf16[512,2048]{1,0:T(8,128)(2,1)} %param.16) | copy-start | bytes 6291460
  6.5 11.2 %copy-start.3 = (f32[8]{0:T(128)S(1)}, f32[8]{0:T(128)}, u32[]{:S(2)}) copy-start(f32[8]{0:T(128)} %param.15) | copy-start | bytes 100
  6.5 67.8 %all-gather.6.cloned.1.call-start = ((), (), s32[]{:S(2)}) async-start(), calls=%async_computation.5 | async-start | bytes 5242880 | tf_op jit(solution)/shard_map/all_gather | solution.py:82
  7.7 9.4 %collective-permute-start.1 = (bf16[128,64]{0,1:T(8,128)(2,1)S(1)}, bf16[128,64]{0,1:T(8,128)(2,1)S(1)}, u32[]{:S(2)}, u32[]{:S(2)}) collective-permute-start(bf16[128,64]{0,1:T(8,128)(2,1)S(1)} %slice.21), channel_id=1, source_target_pairs={{0,4},{4,8},{8,12},{12,16},{16,20},{20,24},{24,28},{1,5},{5,9},{9,... | collective-permute-start | bytes 49160 | tf_op jit(solution)/shard_map/ppermute | solution.py:15
  11.2 7.4 %collective-permute-start = (bf16[128,64]{0,1:T(8,128)(2,1)S(1)}, bf16[128,64]{0,1:T(8,128)(2,1)S(1)}, u32[]{:S(2)}, u32[]{:S(2)}) collective-permute-start(bf16[128,64]{0,1:T(8,128)(2,1)S(1)} %slice.20), channel_id=1, source_target_pairs={{0,4},{4,8},{8,12},{12,16},{16,20},{20,24},{24,28},{1,5},{5,9},{9,... | collective-permute-start | bytes 49160 | tf_op jit(solution)/shard_map/ppermute | solution.py:15
  19.6 1.8 copy-start.1
  21.3 131.6 %all-gather.4.cloned.1.call-start = ((), (), s32[]{:S(2)}) async-start(), calls=%async_computation.3 | async-start | bytes 3932160 | tf_op jit(solution)/shard_map/all_gather | solution.py:100
  153.0 6.3 %copy-start.4 = (bf16[1,2048,1024]{2,1,0:T(8,128)(2,1)S(1)}, bf16[1,2048,1024]{2,1,0:T(8,128)(2,1)}, u32[]{:S(2)}) copy-start(bf16[1,2048,1024]{2,1,0:T(8,128)(2,1)} %param.21) | copy-start | bytes 12582916
  153.0 6.3 %copy-start.6 = (bf16[8,96,2048]{2,1,0:T(8,128)(2,1)S(1)}, bf16[8,96,2048]{2,1,0:T(8,128)(2,1)}, u32[]{:S(2)}) copy-start(bf16[8,96,2048]{2,1,0:T(8,128)(2,1)} %all-gather.4.cloned.1.call-done) | copy-start | bytes 9437188
  159.3 3.8 %copy-start.5 = (bf16[1,1024,2048]{2,1,0:T(8,128)(2,1)S(1)}, bf16[1,1024,2048]{2,1,0:T(8,128)(2,1)}, u32[]{:S(2)}) copy-start(bf16[1,1024,2048]{2,1,0:T(8,128)(2,1)} %param.23) | copy-start | bytes 12582916
  167.9 4.8 %copy-start.2 = (f32[256,2]{0,1:T(2,128)S(1)}, f32[256,2]{0,1:T(2,128)}, u32[]{:S(2)}) copy-start(f32[256,2]{0,1:T(2,128)} %param.20) | copy-start | bytes 6148
  167.9 76.3 %all-to-all-start.1 = ((bf16[8,96,2048]{2,1,0:T(8,128)(2,1)}), bf16[8,96,2048]{2,1,0:T(8,128)(2,1)}, u32[]{:S(2)}, u32[]{:S(2)}) async-start(bf16[8,96,2048]{2,1,0:T(8,128)(2,1)} %bitcast.58), calls=%async_computation.1 | async-start | bytes 6291456 | tf_op jit(solution)/shard_map/all_to_all | solution.py:111
  172.7 120.5 %reduce-scatter.2.cloned.1.call-start = ((), (), s32[]{:S(2)}) async-start(), calls=%async_computation.4 | async-start | bytes 1310720 | tf_op jit(solution)/shard_map/reduce_scatter | solution.py:115
Sparse Core Ops, SparseCore 0:
  21.5 52.8 all-gather.5
  111.3 41.6 all-gather.3
  267.3 25.8 reduce-scatter.1
